TPU v7x, 32 devices: a whole 2x2x4 slice. The times are simulated.
32 devices in a mesh: grp: 2 (over y), sp: 4 (over z), tp: 4 (over x, core).
Axes of the slice: x: 2, y: 2, z: 4, core: 2. Of those that a mesh axis runs over, the one named last changes fastest.
Arguments:
- stream: bfloat16 [12288, 4096], P(('grp', 'sp', 'tp')), parts along dimension 0, may hold values from -6 to 6
- norm_gain: float32 [2, 4096], replicated, may hold values from 0.1 to 1.9
- mix_weight: bfloat16 [2, 4, 1024, 1024], P(None, None, 'sp', 'tp'), may hold values from -0.1875 to 0.1875
- branch_scale: float32 [2, 4096], replicated, may hold values from 0.1 to 1.9
Outputs:
- result: bfloat16 [12288, 4096], P(('grp', 'sp', 'tp')), parts along dimension 0
There are 2 independent parts, one for each index of `grp`. A program takes and returns all parts, laid end to end along the dimension named above; an argument that names none is the same for every part. Nothing has to cross between parts.
All inputs are finite; a program needn't handle non-finite values.
Results may differ from a plain program's by a relative error of at most 0.0056.
Values may be sent and summed in bfloat16 or wider, within the bound.
A program may use at most 128 MiB of HBM per device.

v0:
```python
import jax
import jax.numpy as jnp
from jax import lax
from jax.sharding import PartitionSpec as P

GW = 1024
G = 4
LAYERS = 2
epsilon = 1e-06
window_lengths = (2, 4, 8, 16)
halo_rows = 15


def from_behind(block, axis, distance):
    devices = range(lax.axis_size(axis))
    route = [(i - distance, i) for i in devices if i - distance in devices]
    return lax.ppermute(block, axis, route)


def per_device(stream, norm_gain, mix_weight, branch_scale):
    row_count = stream.shape[0]
    feature_width = stream.shape[1]
    offset = lax.axis_index(("sp", "tp")) * row_count
    counts_base = (offset + lax.iota(jnp.int32, row_count)).astype(jnp.float32) + 1.0
    residual = stream.astype(jnp.float32)
    for layer_idx in range(LAYERS):
        scale_rows = lax.rsqrt(jnp.mean(residual * residual, axis=1, keepdims=True) + epsilon)
        normed = (residual * scale_rows * norm_gain[layer_idx]).astype(jnp.bfloat16)
        earlier = from_behind(normed[row_count - halo_rows :], ("sp", "tp"), 1)
        extended = jnp.concatenate([earlier, normed], axis=0).astype(jnp.float32)
        pieces = []
        for group_idx in range(G):
            window_len = window_lengths[group_idx]
            segment = extended[:, group_idx * GW : (group_idx + 1) * GW]
            own_rows = segment[halo_rows:]
            running = own_rows
            for back_step in range(1, window_len):
                running = (
                    running + segment[halo_rows - back_step : halo_rows - back_step + row_count]
                )
            window_mean = running / jnp.minimum(counts_base, float(window_len))[:, None]
            pieces.append((window_mean - own_rows).astype(jnp.bfloat16))
        pooled = jnp.stack(pieces, axis=1)
        weight_shard = mix_weight[layer_idx]
        full_rows = lax.all_gather(weight_shard, "sp", axis=1, tiled=True)
        mixed_out = jnp.einsum(
            "rgc,gcn->rgn",
            pooled,
            lax.all_gather(full_rows, "tp", axis=2, tiled=True),
            preferred_element_type=jnp.float32,
        )
        residual = residual + mixed_out.reshape(row_count, feature_width) * branch_scale[layer_idx]
    return residual.astype(jnp.bfloat16)


def solution(mesh):
    return jax.shard_map(
        per_device,
        mesh=mesh,
        in_specs=(P(("grp", "sp", "tp"), None), P(), P(None, None, "sp", "tp"), P()),
        out_specs=P(("grp", "sp", "tp"), None),
        check_vma=False,
    )
```

profile of v0, /device:TPU:9, one launch (start us, length us, event | category | flops | bytes accessed | tf_op | source)
XLA Modules:
  0.0 248.3 jit_solution(16958773101239605890)
XLA Ops:
  6.5 0.0 all-gather.9.cloned.1.call-start
  6.5 2.2 fusion.69
  8.8 0.0 copy-start.1
  8.8 0.0 all-gather.9.cloned.1.call-update
  8.8 0.0 all-gather.13.cloned.1.call-start
  8.9 0.7 all-gather.13.cloned.1.call-update
  9.6 0.0 all-gather.11.cloned.1.call-start
  9.6 44.4 %all-gather.9.cloned.1.call-done = bf16[1,4,1024,256]{3,2,1,0:T(8,128)(2,1)} async-done(((bf16[1,4,256,256]{3,2,1,0:T(8,128)(2,1)}), bf16[1,4,1024,256]{3,2,1,0:T(8,128)(2,1)}) %all-gather.9.cloned.1.call-update) | async-done | bytes 2097168 | tf_op jit(solution)/shard_map/all_gather | solution.py:45
  54.0 0.0 all-gather.11.cloned.1.call-update
  54.0 0.0 all-gather.15.cloned.1.call-start
  54.0 0.0 copy-done.1
  54.0 0.7 fusion.4
  54.7 0.0 copy-start.3
  54.8 45.3 %all-gather.13.cloned.1.call-done = bf16[1,4,1024,256]{3,2,1,0:T(8,128)(2,1)} async-done(((bf16[1,4,256,256]{3,2,1,0:T(8,128)(2,1)}), bf16[1,4,1024,256]{3,2,1,0:T(8,128)(2,1)}) %all-gather.13.cloned.1.call-update) | async-done | bytes 2097168 | tf_op jit(solution)/shard_map/all_gather | solution.py:45
  100.0 0.0 all-gather.15.cloned.1.call-update
  100.0 0.0 copy-done.3
  100.1 0.0 copy-start.4
  100.1 1.0 fusion.6
  101.1 0.0 copy-start.2
  101.1 1.7 copy-done.2
  102.8 4.2 %collective-permute-start = (bf16[15,4096]{1,0:T(8,128)(2,1)S(1)}, bf16[15,4096]{1,0:T(8,128)(2,1)S(1)}, u32[]{:S(2)}, u32[]{:S(2)}) collective-permute-start(bf16[15,4096]{1,0:T(8,128)(2,1)S(1)} %slice.340), channel_id=1, source_target_pairs={{0,1},{1,2},{2,3},{3,4},{4,5},{5,6},{6,7},{7,8},{8,9},{9,10},{10,1... | collective-permute-start | bytes 368648 | tf_op jit(solution)/shard_map/ppermute | solution.py:17
  107.0 0.0 copy-done.4
  107.1 1.8 collective-permute-done
  108.9 3.2 %maximum_convert_fusion = f32[399,4096]{1,0:T(8,128)S(1)} fusion(bf16[384,4096]{1,0:T(8,128)(2,1)} %copy-done.2, bf16[15,4096]{1,0:T(8,128)(2,1)S(1)} %collective-permute-done), kind=kLoop, calls=%fused_computation.13 | loop fusion | flops 6537216 | bytes 9805824 | tf_op jit(solution)/shard_map/convert_element_type | solution.py:30
  112.2 3.3 %fusion.62 = bf16[384,1,1024]{2,0,1:T(8,128)(2,1)} fusion(f32[384]{0:T(512)S(1)} %fusion.63, f32[399,4096]{1,0:T(8,128)S(1)} %maximum_convert_fusion), kind=kLoop, calls=%fused_computation.114 | loop fusion | flops 7077888 | bytes 25953792 | tf_op jit(solution)/shard_map/stack | solution.py:43
  115.4 3.6 %fusion.56 = (bf16[384,1,1024]{2,0,1:T(8,128)(2,1)}, bf16[384,1,1024]{2,0,1:T(8,128)(2,1)}, bf16[384,1,1024]{2,0,1:T(8,128)(2,1)}) fusion(f32[384]{0:T(512)S(1)} %fusion.66, f32[399,4096]{1,0:T(8,128)S(1)} %maximum_convert_fusion, f32[384]{0:T(512)S(1)} %get-tuple-element.18, f32[384]{0:T(512)S(1)} %get-tuple-element.17), kind=kLoop, calls=%fused_computation.108 | loop fusion | flops 7864320 | bytes 24384000 | tf_op jit(solution)/shard_map/stack | solution.py:43
  119.0 43.0 %all-gather.11.cloned.1.call-done = bf16[1,4,1024,1024]{3,2,1,0:T(8,128)(2,1)} async-done(((bf16[1,4,1024,256]{3,2,1,0:T(8,128)(2,1)}), bf16[1,4,1024,1024]{3,2,1,0:T(8,128)(2,1)}) %all-gather.11.cloned.1.call-update) | async-done | bytes 8388624 | tf_op jit(solution)/shard_map/all_gather | solution.py:49
  162.0 7.8 %fusion.21 = f32[4,48,8,1024]{3,2,1,0:T(8,128)S(1)} fusion(bf16[1,4,1024,1024]{3,2,1,0:T(8,128)(2,1)} %all-gather.11.cloned.1.call-done, bf16[384,1,1024]{2,0,1:T(8,128)(2,1)} %fusion.62, bf16[384,1,1024]{2,0,1:T(8,128)(2,1)} %get-tuple-element.10, bf16[384,1,1024]{2,0,1:T(8,128)(2,1)} %get-tuple-element.9, bf16[384,1,1024]{2,0,1:T(8,128)(2,1)} %get-tuple-element.8), kind=kOutput, calls=%fused_computation.29 | convolution fusion | flops 3225944064 | bytes 17825792 | tf_op jit(solution)/shard_map/rgc,gcn->rgn/dot_general | solution.py:46
  169.8 0.6 copy.7
  170.4 0.0 copy-start
  170.4 1.2 multiply_reduce_fusion
  171.6 2.0 copy-done
  173.7 1.6 multiply_convert_fusion
  175.3 2.3 collective-permute-start.1
  177.6 4.6 %collective-permute-done.1 = bf16[15,4096]{1,0:T(8,128)(2,1)S(1)} collective-permute-done((bf16[15,4096]{1,0:T(8,128)(2,1)S(1)}, bf16[15,4096]{1,0:T(8,128)(2,1)S(1)}, u32[]{:S(2)}, u32[]{:S(2)}) %collective-permute-start.1) | collective-permute-done | bytes 122912 | tf_op jit(solution)/shard_map/ppermute | solution.py:17
  182.2 0.9 maximum_convert_fusion.1
  183.1 3.3 %fusion.61 = bf16[384,1,1024]{2,0,1:T(8,128)(2,1)} fusion(f32[384]{0:T(512)S(1)} %fusion.63, f32[399,4096]{1,0:T(8,128)S(1)} %maximum_convert_fusion.1), kind=kLoop, calls=%fused_computation.113 | loop fusion | flops 7077888 | bytes 25953792 | tf_op jit(solution)/shard_map/stack | solution.py:43
  186.4 3.5 %fusion.55 = (bf16[384,1,1024]{2,0,1:T(8,128)(2,1)}, bf16[384,1,1024]{2,0,1:T(8,128)(2,1)}, bf16[384,1,1024]{2,0,1:T(8,128)(2,1)}) fusion(f32[384]{0:T(512)S(1)} %fusion.66, f32[399,4096]{1,0:T(8,128)S(1)} %maximum_convert_fusion.1, f32[384]{0:T(512)S(1)} %get-tuple-element.18, f32[384]{0:T(512)S(1)} %get-tuple-element.17), kind=kLoop, calls=%fused_computation.107 | loop fusion | flops 7864320 | bytes 24384000 | tf_op jit(solution)/shard_map/stack | solution.py:43
  189.9 34.3 %all-gather.15.cloned.1.call-done = bf16[1,4,1024,1024]{3,2,1,0:T(8,128)(2,1)} async-done(((bf16[1,4,1024,256]{3,2,1,0:T(8,128)(2,1)}), bf16[1,4,1024,1024]{3,2,1,0:T(8,128)(2,1)}) %all-gather.15.cloned.1.call-update) | async-done | bytes 8388624 | tf_op jit(solution)/shard_map/all_gather | solution.py:49
  224.3 0.0 slice-start
  224.3 0.0 slice-start.1
  224.3 7.9 %fusion.26 = f32[4,48,8,1024]{3,2,1,0:T(8,128)S(1)} fusion(bf16[1,4,1024,1024]{3,2,1,0:T(8,128)(2,1)} %all-gather.15.cloned.1.call-done, bf16[384,1,1024]{2,0,1:T(8,128)(2,1)} %fusion.61, bf16[384,1,1024]{2,0,1:T(8,128)(2,1)} %get-tuple-element.7, bf16[384,1,1024]{2,0,1:T(8,128)(2,1)} %get-tuple-element.6, bf16[384,1,1024]{2,0,1:T(8,128)(2,1)} %get-tuple-element.5), kind=kOutput, calls=%fused_computation.30 | convolution fusion | flops 3225944064 | bytes 17825792 | tf_op jit(solution)/shard_map/rgc,gcn->rgn/dot_general | solution.py:46
  232.2 3.4 %copy.8 = f32[4,48,8,1024]{3,2,0,1:T(8,128)} copy(f32[4,48,8,1024]{3,2,1,0:T(8,128)S(1)} %fusion.26) | data formatting | bytes 12582912 | tf_op jit(solution)/shard_map/reshape | solution.py:52
  235.6 0.0 slice-done
  235.6 0.0 slice-done.1
  235.6 6.2 %add_convert_fusion = bf16[384,4096]{1,0:T(8,128)(2,1)} fusion(f32[384,4096]{1,0:T(8,128)} %bitcast.43, f32[4096]{0:T(1024)S(1)} %bitcast.47, f32[384,4096]{1,0:T(8,128)S(1)} %bitcast.42, f32[4096]{0:T(1024)S(1)} %bitcast.46, bf16[384,4096]{1,0:T(8,128)(2,1)S(1)} %copy-done.1), kind=kLoop, calls=%fused_computation.10 | loop fusion | flops 9437184 | bytes 18907136 | tf_op jit(solution)/shard_map/convert_element_type | solution.py:53
  (10 shorter events, 0.2 us)
Async XLA Ops:
  6.5 47.4 %all-gather.9.cloned.1.call-start = ((), (), s32[]{:S(2)}) async-start(), calls=%async_computation | async-start | bytes 2621440 | tf_op jit(solution)/shard_map/all_gather | solution.py:45
  8.8 45.3 %copy-start.1 = (bf16[384,4096]{1,0:T(8,128)(2,1)S(1)}, bf16[384,4096]{1,0:T(8,128)(2,1)}, u32[]{:S(2)}) copy-start(bf16[384,4096]{1,0:T(8,128)(2,1)} %param.4) | copy-start | bytes 9437188
  8.8 91.2 %all-gather.13.cloned.1.call-start = ((), (), s32[]{:S(2)}) async-start(), calls=%async_computation.2 | async-start | bytes 2621440 | tf_op jit(solution)/shard_map/all_gather | solution.py:45
  9.6 152.5 %all-gather.11.cloned.1.call-start = ((), (), s32[]{:S(2)}) async-start(), calls=%async_computation.1 | async-start | bytes 10485760 | tf_op jit(solution)/shard_map/all_gather | solution.py:49
  54.0 170.3 %all-gather.15.cloned.1.call-start = ((), (), s32[]{:S(2)}) async-start(), calls=%async_computation.3 | async-start | bytes 10485760 | tf_op jit(solution)/shard_map/all_gather | solution.py:49
  54.7 45.3 %copy-start.3 = (f32[2,4096]{1,0:T(2,128)S(1)}, f32[2,4096]{1,0:T(2,128)}, u32[]{:S(2)}) copy-start(f32[2,4096]{1,0:T(2,128)} %param.5) | copy-start | bytes 98308
  100.1 6.9 %copy-start.4 = (f32[2,4096]{1,0:T(2,128)S(1)}, f32[2,4096]{1,0:T(2,128)}, u32[]{:S(2)}) copy-start(f32[2,4096]{1,0:T(2,128)} %param.7) | copy-start | bytes 98308
  101.1 1.7 copy-start.2
  102.8 6.1 %collective-permute-start = (bf16[15,4096]{1,0:T(8,128)(2,1)S(1)}, bf16[15,4096]{1,0:T(8,128)(2,1)S(1)}, u32[]{:S(2)}, u32[]{:S(2)}) collective-permute-start(bf16[15,4096]{1,0:T(8,128)(2,1)S(1)} %slice.340), channel_id=1, source_target_pairs={{0,1},{1,2},{2,3},{3,4},{4,5},{5,6},{6,7},{7,8},{8,9},{9,10},{10,1... | collective-permute-start | bytes 368648 | tf_op jit(solution)/shard_map/ppermute | solution.py:17
  170.4 3.3 %copy-start = (f32[4,48,8,1024]{3,2,0,1:T(8,128)}, f32[4,48,8,1024]{3,2,0,1:T(8,128)S(1)}, u32[]{:S(2)}) copy-start(f32[4,48,8,1024]{3,2,0,1:T(8,128)S(1)} %copy.7) | copy-start | bytes 18874372
  175.3 6.9 %collective-permute-start.1 = (bf16[15,4096]{1,0:T(8,128)(2,1)S(1)}, bf16[15,4096]{1,0:T(8,128)(2,1)S(1)}, u32[]{:S(2)}, u32[]{:S(2)}) collective-permute-start(bf16[15,4096]{1,0:T(8,128)(2,1)S(1)} %slice.371), channel_id=1, source_target_pairs={{0,1},{1,2},{2,3},{3,4},{4,5},{5,6},{6,7},{7,8},{8,9},{9,10},{10,1... | collective-permute-start | bytes 368648 | tf_op jit(solution)/shard_map/ppermute | solution.py:17
  224.3 11.3 %slice-start = ((s8[6291456]{0:T(1024)(128)(4,1)}), s8[4194304]{0:T(1024)(128)(4,1)S(1)}, s32[]{:S(2)}) async-start(s8[6291456]{0:T(1024)(128)(4,1)} %bitcast.40), calls=%async_computation.4 | async-start | bytes 8388608
  224.3 11.3 %slice-start.1 = ((s8[6291456]{0:T(1024)(128)(4,1)}), s8[2097152]{0:T(1024)(128)(4,1)S(1)}, s32[]{:S(2)}) async-start(s8[6291456]{0:T(1024)(128)(4,1)} %bitcast.40), calls=%async_computation.5 | async-start | bytes 4194304
Sparse Core Ops, SparseCore 0:
  8.9 44.9 all-gather.8
  55.5 44.4 all-gather.12
  101.6 60.4 all-gather.10
  163.4 60.7 all-gather.14
where the time goes:
time: 249 us; the launch traced here: 248 us
  waiting for transfers between devices  174 us (70%)
  other arithmetic  28.5 us (11%)
  matrix products  15.6 us (6%)
  between operations  13.3 us (5%)
  local copies, waits for them, and re-layouts  10.1 us (4%)
  starting transfers between devices  6.56 us (3%)
    all_gather x2, waiting for transfers between devices, per_device(): full_rows = lax.all_gather(weight_shard, 'sp', axis=1, tiled=True)  89.6 us
    all_gather x2, waiting for transfers between devices, per_device(): lax.all_gather(full_rows, 'tp', axis=2, tiled=True)  77.3 us
    dot_general x2, matrix products, per_device(): jnp.einsum('rgc,gcn->rgn', pooled, lax.all_gather(full_rows, 'tp', axis=2...  15.6 us
    another operation x4, other arithmetic, per_device(): pooled = jnp.stack(pieces, axis=1)  13.6 us
    ppermute x2, waiting for transfers between devices, from_behind(): return lax.ppermute(block, axis, route)  6.48 us
    ppermute x2, starting transfers between devices, from_behind(): return lax.ppermute(block, axis, route)  6.44 us
    convert_element_type x1, other arithmetic, per_device(): return residual.astype(jnp.bfloat16)  6.2 us
  transfers between devices with their start and end apart: 6, of which 6 were waited for; matrix products, arithmetic and copies ran while one was open for 12% of the time, Pallas kernels for 0%

commit v1 on v0

--- a/solution.py
+++ b/solution.py
@@ -9,6 +9,16 @@
 epsilon = 1e-06
 window_lengths = (2, 4, 8, 16)
 halo_rows = 15
+
+
+def turned_line(shard, axis, dim):
+    size = lax.axis_size(axis)
+    held, shards = (shard, [shard])
+    for _ in range(size - 1):
+        held = lax.ppermute(held, axis, [(i, (i + 1) % size) for i in range(size)])
+        shards.insert(0, held)
+    merged = jnp.concatenate(shards, axis=dim)
+    return jnp.roll(merged, (lax.axis_index(axis) + 1) * shard.shape[dim], axis=dim)
 
 
 def from_behind(block, axis, distance):
@@ -42,7 +52,7 @@
             pieces.append((window_mean - own_rows).astype(jnp.bfloat16))
         pooled = jnp.stack(pieces, axis=1)
         weight_shard = mix_weight[layer_idx]
-        full_rows = lax.all_gather(weight_shard, "sp", axis=1, tiled=True)
+        full_rows = turned_line(weight_shard, "sp", 1)
         mixed_out = jnp.einsum(
             "rgc,gcn->rgn",
             pooled,

time: 249 us -> 208 us (0.84)
  waiting for transfers between devices: 174 us -> 97.9 us
  other arithmetic: 28.5 us -> 41.2 us
  matrix products: 15.6 us -> 23.5 us
  starting transfers between devices: 6.56 us -> 14.3 us
  local copies, waits for them, and re-layouts: 10.1 us -> 17.5 us
    all_gather x2 -> x0, waiting for transfers between devices: 89.6 us -> none  [per_device(): full_rows = lax.all_gather(weight_shard, 'sp', axis=1, tiled=True)]
    ppermute x0 -> x6, waiting for transfers between devices: none -> 71.2 us  [turned_line(): held = lax.ppermute(held, axis, [(i, (i + 1) % size) for i in range(size)])]
    all_gather x2, waiting for transfers between devices: 77.3 us -> 17.6 us  [per_device(): lax.all_gather(full_rows, 'tp', axis=2, tiled=True)]
    reshape x2, local copies, waits for them, and re-layouts: 4.01 us -> 13.4 us  [per_device(): mixed_out.reshape(row_count, feature_width) * branch_scale[layer_idx]]
    concatenate x0 -> x2, other arithmetic: none -> 8.48 us  [turned_line(): jnp.roll(merged, (lax.axis_index(axis) + 1) * shard.shape[dim], axis=dim)]
    dot_general x2, matrix products: 15.6 us -> 23.5 us  [per_device(): jnp.einsum('rgc,gcn->rgn', pooled, lax.all_gather(full_rows, 'tp', axis=2...]
    ppermute x2, starting transfers between devices: 6.44 us -> 11.6 us  [from_behind(): return lax.ppermute(block, axis, route)]
    reduce_sum x2, other arithmetic: 1.92 us -> 4.73 us  [per_device(): jnp.mean(residual * residual, axis=1, keepdims=True) + epsilon]
  transfers between devices with their start and end apart: 6 -> 10, of which waited for: 6 -> 9; matrix products, arithmetic and copies ran while one was open for 12% -> 24% of each run, Pallas kernels for 0% -> 0%
where the time goes in v1:
time: 208 us
  waiting for transfers between devices  97.9 us (47%)
  other arithmetic  41.2 us (20%)
  matrix products  23.5 us (11%)
  local copies, waits for them, and re-layouts  17.5 us (8%)
  starting transfers between devices  14.3 us (7%)
  between operations  13.6 us (7%)
    ppermute x6, waiting for transfers between devices, turned_line(): held = lax.ppermute(held, axis, [(i, (i + 1) % size) for i in range(size)])  71.2 us
    dot_general x2, matrix products, per_device(): jnp.einsum('rgc,gcn->rgn', pooled, lax.all_gather(full_rows, 'tp', axis=2...  23.5 us
    all_gather x2, waiting for transfers between devices, per_device(): lax.all_gather(full_rows, 'tp', axis=2, tiled=True)  17.6 us
    another operation x4, other arithmetic, per_device(): pooled = jnp.stack(pieces, axis=1)  13.7 us
    reshape x2, local copies, waits for them, and re-layouts, per_device(): mixed_out.reshape(row_count, feature_width) * branch_scale[layer_idx]  13.4 us
    ppermute x2, starting transfers between devices, from_behind(): return lax.ppermute(block, axis, route)  11.6 us
    ppermute x2, waiting for transfers between devices, from_behind(): return lax.ppermute(block, axis, route)  9.15 us
    concatenate x2, other arithmetic, turned_line(): jnp.roll(merged, (lax.axis_index(axis) + 1) * shard.shape[dim], axis=dim)  8.48 us
  transfers between devices with their start and end apart: 10, of which 9 were waited for; matrix products, arithmetic and copies ran while one was open for 24% of the time, Pallas kernels for 0%

profile of v1, /device:TPU:9, one launch (start us, length us, event | category | flops | bytes accessed | tf_op | source)
XLA Modules:
  0.0 208.0 jit_solution(7850644226723461569)
XLA Ops:
  6.5 0.0 all-gather.3.cloned.1.call-start
  6.5 1.3 fusion.71
  7.8 0.2 copy.11
  8.0 1.3 collective-permute-start
  9.4 11.5 %collective-permute-done = bf16[4,256,256]{1,2,0:T(8,128)(2,1)S(1)} collective-permute-done((bf16[4,256,256]{1,2,0:T(8,128)(2,1)S(1)}, bf16[4,256,256]{1,2,0:T(8,128)(2,1)S(1)}, u32[]{:S(2)}, u32[]{:S(2)}) %collective-permute-start) | collective-permute-done | bytes 524320 | tf_op jit(solution)/shard_map/ppermute | solution.py:18
  20.9 1.3 collective-permute-start.1
  22.2 12.1 %collective-permute-done.1 = bf16[4,256,256]{1,2,0:T(8,128)(2,1)S(1)} collective-permute-done((bf16[4,256,256]{1,2,0:T(8,128)(2,1)S(1)}, bf16[4,256,256]{1,2,0:T(8,128)(2,1)S(1)}, u32[]{:S(2)}, u32[]{:S(2)}) %collective-permute-start.1) | collective-permute-done | bytes 524320 | tf_op jit(solution)/shard_map/ppermute | solution.py:18
  34.2 0.0 collective-permute-start.2
  34.2 13.2 %collective-permute-done.2 = bf16[4,256,256]{1,2,0:T(8,128)(2,1)S(1)} collective-permute-done((bf16[4,256,256]{1,2,0:T(8,128)(2,1)S(1)}, bf16[4,256,256]{1,2,0:T(8,128)(2,1)S(1)}, u32[]{:S(2)}, u32[]{:S(2)}) %collective-permute-start.2) | collective-permute-done | bytes 524320 | tf_op jit(solution)/shard_map/ppermute | solution.py:18
  47.4 3.6 %fusion.29 = bf16[4,1024,256]{1,2,0:T(8,128)(2,1)} fusion(s32[]{:T(128)S(6)} %select_n.13, bf16[4,256,256]{1,2,0:T(8,128)(2,1)S(1)} %collective-permute-done.2, bf16[4,256,256]{1,2,0:T(8,128)(2,1)S(1)} %collective-permute-done.1, bf16[4,256,256]{1,2,0:T(8,128)(2,1)S(1)} %collective-permute-done, bf16[4,256,256]{1,2,0:T(8,128)(2,1)S(1)} %bitcast.33), kind=kLoop, calls=%fused_computation.53 | loop fusion | flops 16777216 | bytes 4194308 | tf_op jit(solution)/shard_map/jit(_roll_dynamic)/concatenate | solution.py:21
  51.1 0.0 all-gather.3.cloned.1.call-update
  51.1 0.0 all-gather.5.cloned.1.call-start
  51.1 0.2 copy.12
  51.3 0.0 copy-start.3
  51.3 0.1 collective-permute-start.4
  51.4 12.3 %collective-permute-done.4 = bf16[4,256,256]{1,2,0:T(8,128)(2,1)S(1)} collective-permute-done((bf16[4,256,256]{1,2,0:T(8,128)(2,1)S(1)}, bf16[4,256,256]{1,2,0:T(8,128)(2,1)S(1)}, u32[]{:S(2)}, u32[]{:S(2)}) %collective-permute-start.4) | collective-permute-done | bytes 524320 | tf_op jit(solution)/shard_map/ppermute | solution.py:18
  63.7 0.0 collective-permute-start.5
  63.7 11.6 %collective-permute-done.5 = bf16[4,256,256]{1,2,0:T(8,128)(2,1)S(1)} collective-permute-done((bf16[4,256,256]{1,2,0:T(8,128)(2,1)S(1)}, bf16[4,256,256]{1,2,0:T(8,128)(2,1)S(1)}, u32[]{:S(2)}, u32[]{:S(2)}) %collective-permute-start.5) | collective-permute-done | bytes 524320 | tf_op jit(solution)/shard_map/ppermute | solution.py:18
  75.3 0.0 collective-permute-start.6
  75.3 0.0 copy-done.4
  75.3 0.0 copy-done.3
  75.3 10.6 %collective-permute-done.6 = bf16[4,256,256]{1,2,0:T(8,128)(2,1)S(1)} collective-permute-done((bf16[4,256,256]{1,2,0:T(8,128)(2,1)S(1)}, bf16[4,256,256]{1,2,0:T(8,128)(2,1)S(1)}, u32[]{:S(2)}, u32[]{:S(2)}) %collective-permute-start.6) | collective-permute-done | bytes 524320 | tf_op jit(solution)/shard_map/ppermute | solution.py:18
  85.9 4.8 %fusion.22 = bf16[4,1024,256]{1,2,0:T(8,128)(2,1)} fusion(s32[]{:T(128)S(6)} %select_n.13, bf16[4,256,256]{1,2,0:T(8,128)(2,1)S(1)} %collective-permute-done.6, bf16[4,256,256]{1,2,0:T(8,128)(2,1)S(1)} %collective-permute-done.5, bf16[4,256,256]{1,2,0:T(8,128)(2,1)S(1)} %collective-permute-done.4, bf16[4,256,256]{1,2,0:T(8,128)(2,1)} %bitcast.35), kind=kLoop, calls=%fused_computation.46 | loop fusion | flops 16777216 | bytes 4194308 | tf_op jit(solution)/shard_map/jit(_roll_dynamic)/concatenate | solution.py:21
  90.7 0.0 all-gather.5.cloned.1.call-update
  90.8 0.0 copy-done.1
  90.8 0.7 fusion
  91.5 1.0 fusion.2
  92.5 0.0 copy-start.2
  92.5 1.7 copy-done.2
  94.2 7.2 %collective-permute-start.3 = (bf16[15,4096]{1,0:T(8,128)(2,1)S(1)}, bf16[15,4096]{1,0:T(8,128)(2,1)S(1)}, u32[]{:S(2)}, u32[]{:S(2)}) collective-permute-start(bf16[15,4096]{1,0:T(8,128)(2,1)S(1)} %slice.340), channel_id=1, source_target_pairs={{0,1},{1,2},{2,3},{3,4},{4,5},{5,6},{6,7},{7,8},{8,9},{9,10},{10,1... | collective-permute-start | bytes 368648 | tf_op jit(solution)/shard_map/ppermute | solution.py:27
  101.5 4.5 %collective-permute-done.3 = bf16[15,4096]{1,0:T(8,128)(2,1)S(1)} collective-permute-done((bf16[15,4096]{1,0:T(8,128)(2,1)S(1)}, bf16[15,4096]{1,0:T(8,128)(2,1)S(1)}, u32[]{:S(2)}, u32[]{:S(2)}) %collective-permute-start.3) | collective-permute-done | bytes 122912 | tf_op jit(solution)/shard_map/ppermute | solution.py:27
  106.1 2.8 %maximum_convert_fusion = f32[399,4096]{1,0:T(8,128)S(1)} fusion(bf16[384,4096]{1,0:T(8,128)(2,1)} %copy-done.2, bf16[15,4096]{1,0:T(8,128)(2,1)S(1)} %collective-permute-done.3), kind=kLoop, calls=%fused_computation.25 | loop fusion | flops 6537216 | bytes 9805824 | tf_op jit(solution)/shard_map/convert_element_type | solution.py:40
  108.9 3.3 %fusion.64 = bf16[384,1,1024]{2,0,1:T(8,128)(2,1)} fusion(f32[384]{0:T(512)S(1)} %fusion.65, f32[399,4096]{1,0:T(8,128)S(1)} %maximum_convert_fusion), kind=kLoop, calls=%fused_computation.140 | loop fusion | flops 7077888 | bytes 25953792 | tf_op jit(solution)/shard_map/stack | solution.py:53
  112.2 3.5 %fusion.58 = (bf16[384,1,1024]{2,0,1:T(8,128)(2,1)}, bf16[384,1,1024]{2,0,1:T(8,128)(2,1)}, bf16[384,1,1024]{2,0,1:T(8,128)(2,1)}) fusion(f32[384]{0:T(512)S(1)} %fusion.68, f32[399,4096]{1,0:T(8,128)S(1)} %maximum_convert_fusion, f32[384]{0:T(512)S(1)} %get-tuple-element.19, f32[384]{0:T(512)S(1)} %get-tuple-element.18), kind=kLoop, calls=%fused_computation.134 | loop fusion | flops 7864320 | bytes 24384000 | tf_op jit(solution)/shard_map/stack | solution.py:53
  115.7 12.2 %fusion.3 = f32[4,1024,384]{2,1,0:T(8,128)} fusion(bf16[4,1024,1024]{1,2,0:T(8,128)(2,1)} %all-gather.3.cloned.1.call-done, bf16[384,1,1024]{2,0,1:T(8,128)(2,1)} %fusion.64, bf16[384,1,1024]{2,0,1:T(8,128)(2,1)} %get-tuple-element.11, bf16[384,1,1024]{2,0,1:T(8,128)(2,1)} %get-tuple-element.10, bf16[384,1,1024]{2,0,1:T(8,128)(2,1)} %get-tuple-element.9), kind=kOutput, calls=%fused_computation.27 | convolution fusion | flops 3225944064 | bytes 17825792 | tf_op jit(solution)/shard_map/rgc,gcn->rgn/dot_general | solution.py:56
  128.0 6.8 %copy.9 = f32[384,4096]{1,0:T(8,128)} copy(f32[384,4096]{0,1:T(8,128)} %bitcast.30) | data formatting | bytes 12582912 | tf_op jit(solution)/shard_map/reshape | solution.py:62
  134.8 4.0 %multiply_reduce_fusion = f32[384]{0:T(512)S(1)} fusion(f32[384,4096]{1,0:T(8,128)} %copy.9, f32[4096]{0:T(1024)S(1)} %bitcast.36, bf16[384,4096]{1,0:T(8,128)(2,1)S(1)} %copy-done.1), kind=kLoop, calls=%fused_computation.8 | loop fusion | flops 7863936 | bytes 9455104 | tf_op jit(solution)/shard_map/reduce_sum | solution.py:37
  138.9 0.6 copy-done
  139.5 1.6 multiply_convert_fusion
  141.1 4.3 %collective-permute-start.7 = (bf16[15,4096]{1,0:T(8,128)(2,1)S(1)}, bf16[15,4096]{1,0:T(8,128)(2,1)S(1)}, u32[]{:S(2)}, u32[]{:S(2)}) collective-permute-start(bf16[15,4096]{1,0:T(8,128)(2,1)S(1)} %slice.371), channel_id=1, source_target_pairs={{0,1},{1,2},{2,3},{3,4},{4,5},{5,6},{6,7},{7,8},{8,9},{9,10},{10,1... | collective-permute-start | bytes 368648 | tf_op jit(solution)/shard_map/ppermute | solution.py:27
  145.4 4.6 %collective-permute-done.7 = bf16[15,4096]{1,0:T(8,128)(2,1)S(1)} collective-permute-done((bf16[15,4096]{1,0:T(8,128)(2,1)S(1)}, bf16[15,4096]{1,0:T(8,128)(2,1)S(1)}, u32[]{:S(2)}, u32[]{:S(2)}) %collective-permute-start.7) | collective-permute-done | bytes 122912 | tf_op jit(solution)/shard_map/ppermute | solution.py:27
  150.0 0.9 maximum_convert_fusion.1
  150.9 3.3 %fusion.63 = bf16[384,1,1024]{2,0,1:T(8,128)(2,1)} fusion(f32[384]{0:T(512)S(1)} %fusion.65, f32[399,4096]{1,0:T(8,128)S(1)} %maximum_convert_fusion.1), kind=kLoop, calls=%fused_computation.139 | loop fusion | flops 7077888 | bytes 25953792 | tf_op jit(solution)/shard_map/stack | solution.py:53
  154.2 3.6 %fusion.57 = (bf16[384,1,1024]{2,0,1:T(8,128)(2,1)}, bf16[384,1,1024]{2,0,1:T(8,128)(2,1)}, bf16[384,1,1024]{2,0,1:T(8,128)(2,1)}) fusion(f32[384]{0:T(512)S(1)} %fusion.68, f32[399,4096]{1,0:T(8,128)S(1)} %maximum_convert_fusion.1, f32[384]{0:T(512)S(1)} %get-tuple-element.19, f32[384]{0:T(512)S(1)} %get-tuple-element.18), kind=kLoop, calls=%fused_computation.133 | loop fusion | flops 7864320 | bytes 24384000 | tf_op jit(solution)/shard_map/stack | solution.py:53
  157.8 17.6 %all-gather.5.cloned.1.call-done = bf16[4,1024,1024]{1,2,0:T(8,128)(2,1)} async-done(((bf16[4,1024,256]{1,2,0:T(8,128)(2,1)}), bf16[4,1024,1024]{1,2,0:T(8,128)(2,1)}) %all-gather.5.cloned.1.call-update) | async-done | bytes 8388624 | tf_op jit(solution)/shard_map/all_gather | solution.py:59
  175.4 11.3 %fusion.11 = f32[4,1024,384]{2,1,0:T(8,128)} fusion(bf16[4,1024,1024]{1,2,0:T(8,128)(2,1)} %all-gather.5.cloned.1.call-done, bf16[384,1,1024]{2,0,1:T(8,128)(2,1)} %fusion.63, bf16[384,1,1024]{2,0,1:T(8,128)(2,1)} %get-tuple-element.8, bf16[384,1,1024]{2,0,1:T(8,128)(2,1)} %get-tuple-element.7, bf16[384,1,1024]{2,0,1:T(8,128)(2,1)} %get-tuple-element.6), kind=kOutput, calls=%fused_computation.35 | convolution fusion | flops 3225944064 | bytes 17825792 | tf_op jit(solution)/shard_map/rgc,gcn->rgn/dot_general | solution.py:56
  186.6 6.5 %copy.10 = f32[384,4096]{1,0:T(8,128)} copy(f32[384,4096]{0,1:T(8,128)} %bitcast.31) | data formatting | bytes 12582912 | tf_op jit(solution)/shard_map/reshape | solution.py:62
  193.2 8.0 %add_convert_fusion = bf16[384,4096]{1,0:T(8,128)(2,1)} fusion(f32[384,4096]{1,0:T(8,128)} %copy.10, f32[4096]{0:T(1024)S(1)} %bitcast.40, f32[384,4096]{1,0:T(8,128)} %copy.9, f32[4096]{0:T(1024)S(1)} %bitcast.38, bf16[384,4096]{1,0:T(8,128)(2,1)S(1)} %copy-done.1), kind=kLoop, calls=%fused_computation.6 | loop fusion | flops 9437184 | bytes 18907136 | tf_op jit(solution)/shard_map/convert_element_type | solution.py:63
  (15 shorter events, 0.2 us)
Async XLA Ops:
  6.5 109.2 %all-gather.3.cloned.1.call-start = ((), (), s32[]{:S(2)}) async-start(), calls=%async_computation | async-start | bytes 10485760 | tf_op jit(solution)/shard_map/all_gather | solution.py:59
  8.0 12.9 %collective-permute-start = (bf16[4,256,256]{1,2,0:T(8,128)(2,1)S(1)}, bf16[4,256,256]{1,2,0:T(8,128)(2,1)S(1)}, u32[]{:S(2)}, u32[]{:S(2)}) collective-permute-start(bf16[4,256,256]{1,2,0:T(8,128)(2,1)S(1)} %bitcast.32), channel_id=1, source_target_pairs={{0,4},{4,8},{8,12},{12,0},{1,5},{5,9},{9,13},{13,1},{2,6},{6,10},{... | collective-permute-start | bytes 1572872 | tf_op jit(solution)/shard_map/ppermute | solution.py:18
  20.9 13.4 %collective-permute-start.1 = (bf16[4,256,256]{1,2,0:T(8,128)(2,1)S(1)}, bf16[4,256,256]{1,2,0:T(8,128)(2,1)S(1)}, u32[]{:S(2)}, u32[]{:S(2)}) collective-permute-start(bf16[4,256,256]{1,2,0:T(8,128)(2,1)S(1)} %collective-permute-done), channel_id=1, source_target_pairs={{0,4},{4,8},{8,12},{12,0},{1,5},{5,9},{9,13},{13,1},{2,6},{6,10},{... | collective-permute-start | bytes 1572872 | tf_op jit(solution)/shard_map/ppermute | solution.py:18
  34.2 13.2 %collective-permute-start.2 = (bf16[4,256,256]{1,2,0:T(8,128)(2,1)S(1)}, bf16[4,256,256]{1,2,0:T(8,128)(2,1)S(1)}, u32[]{:S(2)}, u32[]{:S(2)}) collective-permute-start(bf16[4,256,256]{1,2,0:T(8,128)(2,1)S(1)} %collective-permute-done.1), channel_id=1, source_target_pairs={{0,4},{4,8},{8,12},{12,0},{1,5},{5,9},{9,13},{13,1},{2,6},{6,10},{... | collective-permute-start | bytes 1572872 | tf_op jit(solution)/shard_map/ppermute | solution.py:18
  51.0 24.2 %copy-start.4 = (f32[2,4096]{1,0:T(2,128)S(1)}, f32[2,4096]{1,0:T(2,128)}, u32[]{:S(2)}) copy-start(f32[2,4096]{1,0:T(2,128)} %param.7) | copy-start | bytes 98308
  51.1 124.3 %all-gather.5.cloned.1.call-start = ((), (), s32[]{:S(2)}) async-start(), calls=%async_computation.1 | async-start | bytes 10485760 | tf_op jit(solution)/shard_map/all_gather | solution.py:59
  51.3 24.0 %copy-start.3 = (bf16[1,4,256,256]{2,3,1,0:T(8,128)(2,1)}, bf16[1,4,256,256]{2,3,1,0:T(8,128)(2,1)S(1)}, u32[]{:S(2)}) copy-start(bf16[1,4,256,256]{2,3,1,0:T(8,128)(2,1)S(1)} %copy.12) | copy-start | bytes 1572868
  51.3 12.4 %collective-permute-start.4 = (bf16[4,256,256]{1,2,0:T(8,128)(2,1)S(1)}, bf16[4,256,256]{1,2,0:T(8,128)(2,1)S(1)}, u32[]{:S(2)}, u32[]{:S(2)}) collective-permute-start(bf16[4,256,256]{1,2,0:T(8,128)(2,1)S(1)} %bitcast.34), channel_id=1, source_target_pairs={{0,4},{4,8},{8,12},{12,0},{1,5},{5,9},{9,13},{13,1},{2,6},{6,10},{... | collective-permute-start | bytes 1572872 | tf_op jit(solution)/shard_map/ppermute | solution.py:18
  63.7 11.6 %collective-permute-start.5 = (bf16[4,256,256]{1,2,0:T(8,128)(2,1)S(1)}, bf16[4,256,256]{1,2,0:T(8,128)(2,1)S(1)}, u32[]{:S(2)}, u32[]{:S(2)}) collective-permute-start(bf16[4,256,256]{1,2,0:T(8,128)(2,1)S(1)} %collective-permute-done.4), channel_id=1, source_target_pairs={{0,4},{4,8},{8,12},{12,0},{1,5},{5,9},{9,13},{13,1},{2,6},{6,10},{... | collective-permute-start | bytes 1572872 | tf_op jit(solution)/shard_map/ppermute | solution.py:18
  75.3 10.6 %collective-permute-start.6 = (bf16[4,256,256]{1,2,0:T(8,128)(2,1)S(1)}, bf16[4,256,256]{1,2,0:T(8,128)(2,1)S(1)}, u32[]{:S(2)}, u32[]{:S(2)}) collective-permute-start(bf16[4,256,256]{1,2,0:T(8,128)(2,1)S(1)} %collective-permute-done.5), channel_id=1, source_target_pairs={{0,4},{4,8},{8,12},{12,0},{1,5},{5,9},{9,13},{13,1},{2,6},{6,10},{... | collective-permute-start | bytes 1572872 | tf_op jit(solution)/shard_map/ppermute | solution.py:18
  85.9 4.9 %copy-start.1 = (bf16[384,4096]{1,0:T(8,128)(2,1)S(1)}, bf16[384,4096]{1,0:T(8,128)(2,1)}, u32[]{:S(2)}) copy-start(bf16[384,4096]{1,0:T(8,128)(2,1)} %param.6) | copy-start | bytes 9437188
  91.5 10.0 %copy-start.5 = (f32[2,4096]{1,0:T(2,128)S(1)}, f32[2,4096]{1,0:T(2,128)}, u32[]{:S(2)}) copy-start(f32[2,4096]{1,0:T(2,128)} %param.9) | copy-start | bytes 98308
  92.5 1.7 copy-start.2
  94.2 11.9 %collective-permute-start.3 = (bf16[15,4096]{1,0:T(8,128)(2,1)S(1)}, bf16[15,4096]{1,0:T(8,128)(2,1)S(1)}, u32[]{:S(2)}, u32[]{:S(2)}) collective-permute-start(bf16[15,4096]{1,0:T(8,128)(2,1)S(1)} %slice.340), channel_id=1, source_target_pairs={{0,1},{1,2},{2,3},{3,4},{4,5},{5,6},{6,7},{7,8},{8,9},{9,10},{10,1... | collective-permute-start | bytes 368648 | tf_op jit(solution)/shard_map/ppermute | solution.py:27
  134.8 4.7 %copy-start = (f32[384,4096]{1,0:T(8,128)S(1)}, f32[384,4096]{1,0:T(8,128)}, u32[]{:S(2)}) copy-start(f32[384,4096]{1,0:T(8,128)} %copy.9) | copy-start | bytes 18874372
  141.1 8.9 %collective-permute-start.7 = (bf16[15,4096]{1,0:T(8,128)(2,1)S(1)}, bf16[15,4096]{1,0:T(8,128)(2,1)S(1)}, u32[]{:S(2)}, u32[]{:S(2)}) collective-permute-start(bf16[15,4096]{1,0:T(8,128)(2,1)S(1)} %slice.371), channel_id=1, source_target_pairs={{0,1},{1,2},{2,3},{3,4},{4,5},{5,6},{6,7},{7,8},{8,9},{9,10},{10,1... | collective-permute-start | bytes 368648 | tf_op jit(solution)/shard_map/ppermute | solution.py:27
Sparse Core Ops, SparseCore 0:
  51.2 62.8 all-gather.2
  115.7 59.6 all-gather.4
